TPU v7x, 256 devices: a whole 4x4x8 slice. The times are simulated.
256 devices in a mesh: sp: 64 (over z, x, core), tp: 4 (over y).
Axes of the slice: x: 4, y: 4, z: 8, core: 2. Of those that a mesh axis runs over, the one named last changes fastest.
Arguments:
- stream: bfloat16 [32768, 2048], P(('sp', 'tp')), may hold values from -6 to 6
- pool_in: bfloat16 [32768, 1024], P('sp', 'tp'), may hold values from -6 to 6
- doc_ids: int32 [32768], P('sp'), may hold values from 0 to 7, never falling along the last dimension, each value on 1 to 8192 neighbouring positions
- pool_map: bfloat16 [4, 256, 512], P('tp'), may hold values from -0.375 to 0.375
- pool_scale: float32 [2048], P('tp'), may hold values from 0.1 to 1.9
- out_weight: bfloat16 [2048, 2048], P('tp'), may hold values from -0.125 to 0.125
- norm_gain: float32 [2048], replicated, may hold values from 0.1 to 1.9
- routes: int32 [32768, 2], P('sp'), may hold values from 0 to 63, all different within a row; in each aligned block of 128 rows (0 to 127, 128 to 255, ...) at most 6 rows name the same one
- route_weight: float32 [32768, 2], P(('sp', 'tp')), may hold values from 0.2 to 1
- expert_gate: bfloat16 [64, 2048, 1024], P('sp', None, 'tp'), may hold values from -0.125 to 0.125
- expert_up: bfloat16 [64, 2048, 1024], P('sp', None, 'tp'), may hold values from -0.125 to 0.125
- expert_down: bfloat16 [64, 1024, 2048], P('sp', 'tp'), may hold values from -0.1875 to 0.1875
Outputs:
- result: bfloat16 [32768, 2048], P(('sp', 'tp'))
Inputs may be any that keep to these rules, and one draw needn't show every extreme that they name: `routes`: each token names 2 different experts; in each aligned block of 128 rows no expert is named by more than 6 rows, a bound that some block reaches. `doc_ids`: never falling; each document holds at most 8192 positions.
All inputs are finite; a program needn't handle non-finite values.
Results may differ from a plain program's by a relative error of at most 0.014.
Values may be sent and summed in bfloat16 or wider, within the bound.
No kernel may reach another device: no remote copies, remote signals or barrier semaphores. Data moves between devices by JAX's collectives and lax.ppermute only.
A program may use at most 64 MiB of HBM per device.

v0:
```python
import jax
import jax.numpy as jnp
from jax import lax
from jax.sharding import PartitionSpec as P

SPAN = 16
EPS = 1e-06


def passed_along(value, axis, by):
    length = lax.axis_size(axis)
    pairs = [(i, i + by) for i in range(length) if 0 <= i + by < length]
    return lax.ppermute(value, axis, pairs)


def cut_along(value, dim, length):
    before, after = (value.shape[:dim], value.shape[dim + 1 :])
    return jnp.moveaxis(value.reshape(*before, length, -1, *after), dim, 0)


def sum_at_owner(value, axis, dim):
    length = lax.axis_size(axis)
    tiles = lax.all_to_all(cut_along(value, dim, length), axis, 0, 0, tiled=True)
    return jnp.sum(tiles.astype(jnp.float32), axis=0)


def slot_table(route_block, expert_count, capacity, top_count):
    flattened = route_block.reshape(-1)
    one_hot = (flattened[:, None] == jnp.arange(expert_count, dtype=jnp.int32)[None, :]).astype(
        jnp.int32
    )
    ranking = jnp.sum((jnp.cumsum(one_hot, axis=0) - one_hot) * one_hot, axis=1)
    target_slot = flattened * capacity + ranking
    matches = target_slot[None, :] == jnp.arange(expert_count * capacity, dtype=jnp.int32)[:, None]
    sources = jnp.sum(
        jnp.where(matches, jnp.arange(flattened.shape[0], dtype=jnp.int32)[None, :], 0), axis=1
    )
    filled = jnp.any(matches, axis=1)
    return (target_slot, sources // top_count, filled)


def per_device(
    stream,
    pool_in,
    doc_ids,
    pool_map,
    pool_scale,
    out_weight,
    norm_gain,
    routes,
    route_weight,
    expert_gate,
    expert_up,
    expert_down,
):
    row_count = pool_in.shape[0]
    model_width = stream.shape[1]
    top_count = routes.shape[1]
    tp_count = lax.axis_size("tp")
    expert_count = lax.axis_size("sp")
    quarter = row_count // tp_count
    capacity = max(2, 3 * top_count * quarter // (2 * expert_count))
    reach_rows = SPAN - 1
    tail_rows = (
        pool_in[row_count - reach_rows :],
        doc_ids[row_count - reach_rows :].astype(jnp.bfloat16),
    )
    prior_rows, prior_docs = passed_along((tail_rows[0], tail_rows[1]), "sp", 1)
    extended = jnp.concatenate([prior_rows, pool_in], axis=0).astype(jnp.float32)
    extended_docs = jnp.concatenate([prior_docs.astype(jnp.float32), doc_ids.astype(jnp.float32)])
    own_docs = doc_ids.astype(jnp.float32)
    window = jnp.left_shift(jnp.int32(2), lax.axis_index("tp"))
    positions = lax.axis_index("sp") * row_count + jnp.arange(row_count, dtype=jnp.int32)
    running = jnp.zeros(pool_in.shape, jnp.float32)
    counts = jnp.zeros((row_count,), jnp.float32)
    for offset in range(reach_rows + 1):
        begin_row = reach_rows - offset
        piece_rows = extended[begin_row : begin_row + row_count]
        piece_docs = extended_docs[begin_row : begin_row + row_count]
        in_window = (offset < window) & (positions - offset >= 0) & (piece_docs == own_docs)
        running = running + jnp.where(in_window[:, None], piece_rows, 0.0)
        counts = counts + in_window.astype(jnp.float32)
    pooled = (running / counts[:, None] - pool_in.astype(jnp.float32)).astype(jnp.bfloat16)
    branch = (jnp.dot(pooled, pool_map[0], preferred_element_type=jnp.float32) * pool_scale).astype(
        jnp.bfloat16
    )
    projected = sum_at_owner(
        jnp.dot(branch, out_weight, preferred_element_type=jnp.float32).astype(jnp.bfloat16),
        "tp",
        0,
    )
    mixed_rows = (stream.astype(jnp.float32) + projected).astype(jnp.bfloat16)
    mixed_up = mixed_rows.astype(jnp.float32)
    normed = (
        mixed_up * lax.rsqrt(jnp.mean(mixed_up * mixed_up, axis=1, keepdims=True) + EPS) * norm_gain
    ).astype(jnp.bfloat16)
    own_routes = lax.dynamic_slice_in_dim(routes, lax.axis_index("tp") * quarter, quarter, 0)
    own_slots, own_sources, own_filled = slot_table(own_routes, expert_count, capacity, top_count)
    token_index = own_sources.reshape(expert_count, 1, capacity)
    filled_slots = own_filled.reshape(expert_count, 1, capacity)
    dispatch = jnp.where(filled_slots[..., None], normed[token_index], jnp.zeros((), jnp.bfloat16))
    arrived = lax.all_to_all(dispatch, "sp", split_axis=0, concat_axis=0, tiled=True)
    arrived = lax.all_gather(arrived, "tp", axis=1, tiled=True)
    stacked = arrived.reshape(-1, model_width)
    gate_pre = jnp.dot(stacked, expert_gate[0], preferred_element_type=jnp.float32)
    up_pre = jnp.dot(stacked, expert_up[0], preferred_element_type=jnp.float32)
    hidden = (jax.nn.silu(gate_pre) * up_pre).astype(jnp.bfloat16)
    partial_out = jnp.dot(hidden, expert_down[0], preferred_element_type=jnp.float32).reshape(
        arrived.shape
    )
    summed = sum_at_owner(partial_out.astype(jnp.bfloat16), "tp", 1).astype(jnp.bfloat16)
    returned = lax.all_to_all(summed, "sp", split_axis=0, concat_axis=0, tiled=True)
    outputs = returned.reshape(expert_count * capacity, model_width)
    picked = outputs[own_slots].astype(jnp.float32).reshape(quarter, top_count, model_width)
    combined = jnp.sum(route_weight[:, :, None] * picked, axis=1)
    return (mixed_up + combined).astype(jnp.bfloat16)


def solution(mesh):
    in_specs = (
        P(("sp", "tp"), None),
        P("sp", "tp"),
        P("sp"),
        P("tp", None, None),
        P("tp"),
        P("tp", None),
        P(),
        P("sp", None),
        P(("sp", "tp"), None),
        P("sp", None, "tp"),
        P("sp", None, "tp"),
        P("sp", "tp", None),
    )
    out_specs = P(("sp", "tp"), None)
    return jax.shard_map(
        per_device, mesh=mesh, in_specs=in_specs, out_specs=out_specs, check_vma=False
    )
```

profile of v0, /device:TPU:2, one launch (start us, length us, event | category | flops | bytes accessed | tf_op | source)
XLA Modules:
  0.0 378.5 jit_solution(2949899418363238842)
XLA Ops:
  6.5 0.0 copy-start
  6.5 0.9 fusion.128
  7.4 0.1 slice.108
  7.5 1.9 collective-permute-start.1
  9.4 0.7 slice.106
  10.1 3.5 collective-permute-start
  13.6 0.0 collective-permute-done.1
  13.6 0.1 pad_maximum_fusion
  13.7 0.8 convert_add_fusion.1
  14.5 0.5 collective-permute-done
  15.0 1.0 maximum_convert_fusion
  16.1 0.0 copy-done
  16.1 5.4 %convolution_convert_fusion = bf16[512,2048]{1,0:T(8,128)(2,1)} fusion(bf16[512,2048]{1,0:T(8,128)(2,1)S(1)} %copy-done, f32[512]{0:T(512)} %param.16, bf16[512,256]{1,0:T(8,128)(2,1)} %param.13, f32[527,256]{1,0:T(8,128)S(1)} %maximum_convert_fusion, bf16[1,256,512]{2,1,0:T(8,128)(2,1)} %param.15, f32[512]{0:T(512)S(1)} %get-tuple-element.9, ...), kind=kOutput, calls=%fused_computation.5 | convolution fusion | flops 1214119936 | bytes 13119488 | tf_op jit(solution)/shard_map/dot_general | solution.py:88
  21.5 4.5 %all-to-all-start = ((bf16[4,128,2048]{2,1,0:T(8,128)(2,1)}), bf16[4,128,2048]{2,1,0:T(8,128)(2,1)S(1)}, u32[]{:S(2)}, u32[]{:S(2)}) async-start(bf16[4,128,2048]{2,1,0:T(8,128)(2,1)} %bitcast.58), calls=%async_computation | async-start | bytes 4194304 | tf_op jit(solution)/shard_map/all_to_all | solution.py:23
  25.9 0.0 all-gather.2.cloned.1.call-start
  25.9 0.7 broadcast_multiply_fusion
  26.7 0.1 copy.35
  26.8 0.1 eq.103
  26.9 0.1 reshape.209
  27.1 0.6 reduce-window.6
  27.7 0.2 slice_reduce_fusion
  27.9 0.1 fusion.73
  28.0 0.2 select_reduce_fusion
  28.2 0.1 reduce_sum.67
  28.4 0.1 reshape.217
  28.5 0.2 fusion.30
  28.7 0.2 broadcast_in_dim.172
  28.8 0.0 copy-start.5
  28.9 23.3 %all-to-all-done = bf16[4,128,2048]{2,1,0:T(8,128)(2,1)S(1)} async-done(((bf16[4,128,2048]{2,1,0:T(8,128)(2,1)}), bf16[4,128,2048]{2,1,0:T(8,128)(2,1)S(1)}, u32[]{:S(2)}, u32[]{:S(2)}) %all-to-all-start) | async-done | bytes 2097184 | tf_op jit(solution)/shard_map/all_to_all | solution.py:23
  52.1 0.4 convert_reduce_fusion
  52.5 0.0 copy-done.4
  52.5 0.3 fusion.2
  52.8 0.2 fusion.4
  53.0 2.5 gather_fusion
  55.4 1.6 reshape.216
  57.1 1.8 select_bitcast_fusion
  58.9 62.8 %all_to_all.20 = bf16[64,1,6,2048]{3,2,1,0:T(8,128)(2,1)S(1)} all-to-all(bf16[64,1,6,2048]{3,2,1,0:T(8,128)(2,1)S(1)} %select_bitcast_fusion), channel_id=1, replica_groups=mesh['sp'=64,'tp'=4] {'sp'}, dimensions={0} | all-to-all | bytes 3145728 | tf_op jit(solution)/shard_map/all_to_all | solution.py:102
  121.7 2.0 copy.39
  123.7 0.0 all-gather.2.cloned.1.call-update
  123.7 62.7 %all-gather.2.cloned.1.call-done = bf16[64,4,6,2048]{3,0,2,1:T(8,128)(2,1)} async-done(((bf16[64,1,6,2048]{3,0,2,1:T(8,128)(2,1)}), bf16[64,4,6,2048]{3,0,2,1:T(8,128)(2,1)}) %all-gather.2.cloned.1.call-update) | async-done | bytes 6291472 | tf_op jit(solution)/shard_map/all_gather | solution.py:103
  186.4 9.6 %copy.40 = bf16[64,4,6,2048]{3,2,1,0:T(8,128)(2,1)} copy(bf16[64,4,6,2048]{3,0,2,1:T(8,128)(2,1)} %all-gather.2.cloned.1.call-done) | data formatting | bytes 12582912 | tf_op jit(solution)/shard_map/all_gather | solution.py:103
  196.0 11.1 %reshape.211 = bf16[1536,2048]{1,0:T(8,128)(2,1)} reshape(bf16[64,4,6,2048]{3,2,1,0:T(8,128)(2,1)} %copy.40) | data formatting | bytes 12582912 | tf_op jit(solution)/shard_map/reshape | solution.py:104
  207.2 4.8 %fusion.8 = f32[1536,256]{1,0:T(8,128)S(1)} fusion(bf16[1536,2048]{1,0:T(8,128)(2,1)} %reshape.211, bf16[1,2048,256]{2,1,0:T(8,128)(2,1)S(1)} %copy-done.7), kind=kOutput, calls=%fused_computation.21 | convolution fusion | flops 1610612736 | bytes 8912896 | tf_op jit(solution)/shard_map/dot_general | solution.py:105
  212.0 0.0 copy-done.2
  212.0 0.0 copy-done.8
  212.0 2.1 fusion
  214.1 0.0 copy-start.3
  214.1 0.3 dot_general.21
  214.4 0.9 copy-done.3
  215.3 2.0 convert_bitcast_fusion
  217.4 74.6 %all_to_all.21 = bf16[4,64,1,6,2048]{4,1,3,2,0:T(8,128)(2,1)S(1)} all-to-all(bf16[4,64,1,6,2048]{4,1,3,2,0:T(8,128)(2,1)S(1)} %convert_bitcast_fusion), channel_id=1, replica_groups=mesh['sp'=64,'tp'=4] {'tp'}, dimensions={0} | all-to-all | bytes 12582912 | tf_op jit(solution)/shard_map/all_to_all | solution.py:23
  291.9 1.2 bitcast_reduce_fusion
  293.2 2.2 copy.44
  295.4 10.9 %all-to-all-start.3 = ((bf16[64,1,6,2048]{3,2,1,0:T(8,128)(2,1)}), bf16[64,1,6,2048]{3,2,1,0:T(8,128)(2,1)}, u32[]{:S(2)}, u32[]{:S(2)}) async-start(bf16[64,1,6,2048]{3,2,1,0:T(8,128)(2,1)} %copy.44), calls=%async_computation.3 | async-start | bytes 4194304 | tf_op jit(solution)/shard_map/all_to_all | solution.py:112
  306.2 0.1 copy.45
  306.3 0.1 mul.92
  306.5 0.0 copy-done.6
  306.5 0.1 copy.34
  306.6 50.8 %all-to-all-done.3 = bf16[64,1,6,2048]{3,2,1,0:T(8,128)(2,1)} async-done(((bf16[64,1,6,2048]{3,2,1,0:T(8,128)(2,1)}), bf16[64,1,6,2048]{3,2,1,0:T(8,128)(2,1)}, u32[]{:S(2)}, u32[]{:S(2)}) %all-to-all-start.3) | async-done | bytes 1572896 | tf_op jit(solution)/shard_map/all_to_all | solution.py:112
  357.4 2.6 reshape.213
  360.0 2.3 gather_fusion.1
  362.3 3.5 reshape.214
  365.9 4.8 %multiply_reduce_fusion = f32[128,2048]{1,0:T(8,128)S(1)} fusion(f32[128,2,2048]{2,1,0:T(2,128)} %reshape.214, f32[128,2]{1,0:T(8,128)S(1)} %copy.34), kind=kLoop, calls=%fused_computation.8 | loop fusion | flops 786432 | bytes 3146752 | tf_op jit(solution)/shard_map/reduce_sum | solution.py:115
  370.7 0.9 fusion.5
  (19 shorter events, 0.1 us)
Async XLA Ops:
  6.5 9.5 %copy-start = (bf16[512,2048]{1,0:T(8,128)(2,1)S(1)}, bf16[512,2048]{1,0:T(8,128)(2,1)}, u32[]{:S(2)}) copy-start(bf16[512,2048]{1,0:T(8,128)(2,1)} %param.17) | copy-start | bytes 6291460
  7.5 6.2 %collective-permute-start.1 = (bf16[15]{0:T(256)(128)(2,1)S(1)}, bf16[15]{0:T(256)(128)(2,1)S(1)}, u32[]{:S(2)}, u32[]{:S(2)}) collective-permute-start(bf16[15]{0:T(256)(128)(2,1)S(1)} %slice.108), channel_id=1, source_target_pairs={{0,4},{4,8},{8,12},{12,16},{16,20},{20,24},{24,28},{28,32},{32,36}... | collective-permute-start | bytes 98 | tf_op jit(solution)/shard_map/ppermute | solution.py:13
  10.1 5.0 %collective-permute-start = (bf16[15,256]{1,0:T(8,128)(2,1)S(1)}, bf16[15,256]{1,0:T(8,128)(2,1)S(1)}, u32[]{:S(2)}, u32[]{:S(2)}) collective-permute-start(bf16[15,256]{1,0:T(8,128)(2,1)S(1)} %slice.106), channel_id=1, source_target_pairs={{0,4},{4,8},{8,12},{12,16},{16,20},{20,24},{24,28},{28,32},{32,36}... | collective-permute-start | bytes 23048 | tf_op jit(solution)/shard_map/ppermute | solution.py:13
  21.5 30.6 %all-to-all-start = ((bf16[4,128,2048]{2,1,0:T(8,128)(2,1)}), bf16[4,128,2048]{2,1,0:T(8,128)(2,1)S(1)}, u32[]{:S(2)}, u32[]{:S(2)}) async-start(bf16[4,128,2048]{2,1,0:T(8,128)(2,1)} %bitcast.58), calls=%async_computation | async-start | bytes 4194304 | tf_op jit(solution)/shard_map/all_to_all | solution.py:23
  25.9 26.6 %copy-start.4 = (bf16[128,2048]{1,0:T(8,128)(2,1)S(1)}, bf16[128,2048]{1,0:T(8,128)(2,1)}, u32[]{:S(2)}) copy-start(bf16[128,2048]{1,0:T(8,128)(2,1)} %param.12) | copy-start | bytes 1572868
  25.9 160.5 %all-gather.2.cloned.1.call-start = ((), (), s32[]{:S(2)}) async-start(), calls=%async_computation.4 | async-start | bytes 7864320 | tf_op jit(solution)/shard_map/all_gather | solution.py:103
  28.8 23.9 %copy-start.5 = (f32[2048]{0:T(1024)S(1)}, f32[2048]{0:T(1024)}, u32[]{:S(2)}) copy-start(f32[2048]{0:T(1024)} %param.18) | copy-start | bytes 24580
  196.0 11.1 %copy-start.7 = (bf16[1,2048,256]{2,1,0:T(8,128)(2,1)S(1)}, bf16[1,2048,256]{2,1,0:T(8,128)(2,1)}, u32[]{:S(2)}) copy-start(bf16[1,2048,256]{2,1,0:T(8,128)(2,1)} %param.21) | copy-start | bytes 3145732
  207.2 4.8 %copy-start.2 = (bf16[1536,2048]{1,0:T(8,128)(2,1)S(1)}, bf16[1536,2048]{1,0:T(8,128)(2,1)}, u32[]{:S(2)}) copy-start(bf16[1536,2048]{1,0:T(8,128)(2,1)} %reshape.211) | copy-start | bytes 18874372
  207.2 4.9 %copy-start.8 = (bf16[1,2048,256]{2,1,0:T(8,128)(2,1)S(1)}, bf16[1,2048,256]{2,1,0:T(8,128)(2,1)}, u32[]{:S(2)}) copy-start(bf16[1,2048,256]{2,1,0:T(8,128)(2,1)} %param.22) | copy-start | bytes 3145732
  214.1 1.2 copy-start.3
  295.4 11.1 %copy-start.6 = (f32[128,2]{0,1:T(2,128)S(1)}, f32[128,2]{0,1:T(2,128)}, u32[]{:S(2)}) copy-start(f32[128,2]{0,1:T(2,128)} %param.20) | copy-start | bytes 3076
  295.4 62.0 %all-to-all-start.3 = ((bf16[64,1,6,2048]{3,2,1,0:T(8,128)(2,1)}), bf16[64,1,6,2048]{3,2,1,0:T(8,128)(2,1)}, u32[]{:S(2)}, u32[]{:S(2)}) async-start(bf16[64,1,6,2048]{3,2,1,0:T(8,128)(2,1)} %copy.44), calls=%async_computation.3 | async-start | bytes 4194304 | tf_op jit(solution)/shard_map/all_to_all | solution.py:112
  362.3 9.3 %copy-start.1 = (bf16[512,2048]{1,0:T(8,128)(2,1)S(1)}, bf16[512,2048]{1,0:T(8,128)(2,1)}, u32[]{:S(2)}) copy-start(bf16[512,2048]{1,0:T(8,128)(2,1)} %param.17) | copy-start | bytes 6291460
Sparse Core Ops, SparseCore 0:
  123.8 62.5 all-gather.1
where the time goes:
time: 379 us; the launch traced here: 378 us
  waiting for transfers between devices  137 us (36%)
  blocking collectives  137 us (36%)
  local copies, waits for them, and re-layouts  40.9 us (11%)
  starting transfers between devices  20.7 us (5%)
  matrix products  14.3 us (4%)
  other arithmetic  14.2 us (4%)
  between operations  13.7 us (4%)
    all_to_all x1, blocking collectives, sum_at_owner(): lax.all_to_all(cut_along(value, dim, length), axis, 0, 0, tiled=True)  74.6 us
    all_to_all x1, blocking collectives, per_device(): lax.all_to_all(dispatch, 'sp', split_axis=0, concat_axis=0, tiled=True)  62.8 us
    all_gather x1, waiting for transfers between devices, per_device(): arrived = lax.all_gather(arrived, 'tp', axis=1, tiled=True)  62.7 us
    all_to_all x1, waiting for transfers between devices, per_device(): lax.all_to_all(summed, 'sp', split_axis=0, concat_axis=0, tiled=True)  50.8 us
    all_to_all x1, waiting for transfers between devices, sum_at_owner(): lax.all_to_all(cut_along(value, dim, length), axis, 0, 0, tiled=True)  23.3 us
    reshape x1, local copies, waits for them, and re-layouts, per_device(): stacked = arrived.reshape(-1, model_width)  11.1 us
    all_to_all x1, starting transfers between devices, per_device(): lax.all_to_all(summed, 'sp', split_axis=0, concat_axis=0, tiled=True)  10.9 us
    all_gather x1, local copies, waits for them, and re-layouts, per_device(): arrived = lax.all_gather(arrived, 'tp', axis=1, tiled=True)  9.61 us
  transfers between devices with their start and end apart: 5, of which 4 were waited for; matrix products, arithmetic and copies ran while one was open for 1% of the time, Pallas kernels for 0%

commit v1 on v0

--- a/solution.py
+++ b/solution.py
@@ -100,7 +100,22 @@
     filled_slots = own_filled.reshape(expert_count, 1, capacity)
     dispatch = jnp.where(filled_slots[..., None], normed[token_index], jnp.zeros((), jnp.bfloat16))
     arrived = lax.all_to_all(dispatch, "sp", split_axis=0, concat_axis=0, tiled=True)
-    arrived = lax.all_gather(arrived, "tp", axis=1, tiled=True)
+    size, index, rows = (lax.axis_size("tp"), lax.axis_index("tp"), arrived.shape[1])
+    right = [(i_2, (i_2 + 1) % size) for i_2 in range(size)]
+    left = [(i_2, (i_2 - 1) % size) for i_2 in range(size)]
+    out = jnp.zeros((*arrived.shape[:1], size * rows, *arrived.shape[1 + 1 :]), arrived.dtype)
+    out = lax.dynamic_update_slice_in_dim(out, arrived, index * rows, axis=1)
+    from_left = from_right = arrived
+    half = size // 2
+    for hop in range(1, half + 1):
+        from_left = lax.ppermute(from_left, "tp", right)
+        out = lax.dynamic_update_slice_in_dim(out, from_left, (index - hop) % size * rows, axis=1)
+        if hop < size - half:
+            from_right = lax.ppermute(from_right, "tp", left)
+            out = lax.dynamic_update_slice_in_dim(
+                out, from_right, (index + hop) % size * rows, axis=1
+            )
+    arrived = out
     stacked = arrived.reshape(-1, model_width)
     gate_pre = jnp.dot(stacked, expert_gate[0], preferred_element_type=jnp.float32)
     up_pre = jnp.dot(stacked, expert_up[0], preferred_element_type=jnp.float32)

time: 379 us -> 367 us (0.968)
  between operations: 13.7 us -> 0.31 us
  local copies, waits for them, and re-layouts: 40.9 us -> 48 us
  waiting for transfers between devices: 137 us -> 130 us
  starting transfers between devices: 20.7 us -> 25.4 us
    all_gather x1 -> x0, waiting for transfers between devices: 62.7 us -> none  [per_device(): arrived = lax.all_gather(arrived, 'tp', axis=1, tiled=True)]
    ppermute x0 -> x3, waiting for transfers between devices: none -> 55.2 us  [the longest x2 55.2 us: per_device(): from_left = lax.ppermute(from_left, 'tp', right)]
    dynamic_update_slice x0 -> x4, local copies, waits for them, and re-layouts: none -> 12.3 us  [the longest x2 7.2 us: per_device(): lax.dynamic_update_slice_in_dim(out, from_left, (index - hop) % size * ro...]
    all_gather x1 -> x0, local copies, waits for them, and re-layouts: 9.61 us -> none  [per_device(): arrived = lax.all_gather(arrived, 'tp', axis=1, tiled=True)]
    broadcast_in_dim x0 -> x1, local copies, waits for them, and re-layouts: none -> 4.29 us  [per_device(): jnp.zeros((*arrived.shape[:1], size * rows, *arrived.shape[1 + 1:]), arri...]
  transfers between devices with their start and end apart: 5 -> 7, of which waited for: 4 -> 5; matrix products, arithmetic and copies ran while one was open for 1% -> 5% of each run, Pallas kernels for 0% -> 0%
where the time goes in v1:
time: 367 us; the launch traced here: 366 us
  blocking collectives  134 us (37%)
  waiting for transfers between devices  130 us (35%)
  local copies, waits for them, and re-layouts  48 us (13%)
  starting transfers between devices  25.4 us (7%)
  matrix products  14.3 us (4%)
  other arithmetic  14.2 us (4%)
    all_to_all x1, blocking collectives, sum_at_owner(): lax.all_to_all(cut_along(value, dim, length), axis, 0, 0, tiled=True)  71 us
    all_to_all x1, blocking collectives, per_device(): lax.all_to_all(dispatch, 'sp', split_axis=0, concat_axis=0, tiled=True)  62.8 us
    ppermute x2, waiting for transfers between devices, per_device(): from_left = lax.ppermute(from_left, 'tp', right)  55.2 us
    all_to_all x1, waiting for transfers between devices, per_device(): lax.all_to_all(summed, 'sp', split_axis=0, concat_axis=0, tiled=True)  50.8 us
    all_to_all x1, waiting for transfers between devices, sum_at_owner(): lax.all_to_all(cut_along(value, dim, length), axis, 0, 0, tiled=True)  23.3 us
    all_to_all x1, starting transfers between devices, per_device(): lax.all_to_all(summed, 'sp', split_axis=0, concat_axis=0, tiled=True)  12.3 us
    reshape x1, local copies, waits for them, and re-layouts, per_device(): stacked = arrived.reshape(-1, model_width)  11.1 us
  transfers between devices with their start and end apart: 7, of which 5 were waited for; matrix products, arithmetic and copies ran while one was open for 5% of the time, Pallas kernels for 0%

profile of v1, /device:TPU:2, one launch (start us, length us, event | category | flops | bytes accessed | tf_op | source)
XLA Modules:
  0.0 365.7 jit_solution(7192263257635174421)
XLA Ops:
  0.0 0.9 fusion.130
  0.9 0.1 slice.108
  0.9 1.9 collective-permute-start.1
  2.8 0.7 slice.106
  3.6 3.5 collective-permute-start
  7.1 0.1 pad_maximum_fusion
  7.2 0.8 convert_add_fusion.1
  8.0 0.5 collective-permute-done
  8.5 1.0 maximum_convert_fusion
  9.5 5.4 %convolution_convert_fusion = bf16[512,2048]{1,0:T(8,128)(2,1)} fusion(bf16[512,2048]{1,0:T(8,128)(2,1)S(1)} %copy-done, f32[512]{0:T(512)} %param.16, bf16[512,256]{1,0:T(8,128)(2,1)} %param.13, f32[527,256]{1,0:T(8,128)S(1)} %maximum_convert_fusion, bf16[1,256,512]{2,1,0:T(8,128)(2,1)} %param.15, f32[512]{0:T(512)S(1)} %get-tuple-element.9, ...), kind=kOutput, calls=%fused_computation.5 | convolution fusion | flops 1214119936 | bytes 13119488 | tf_op jit(solution)/shard_map/dot_general | solution.py:88
  14.9 4.5 %all-to-all-start = ((bf16[4,128,2048]{2,1,0:T(8,128)(2,1)}), bf16[4,128,2048]{2,1,0:T(8,128)(2,1)S(1)}, u32[]{:S(2)}, u32[]{:S(2)}) async-start(bf16[4,128,2048]{2,1,0:T(8,128)(2,1)} %bitcast.60), calls=%async_computation | async-start | bytes 4194304 | tf_op jit(solution)/shard_map/all_to_all | solution.py:23
  19.4 0.7 broadcast_multiply_fusion
  20.1 0.1 copy.41
  20.3 0.1 eq.107
  20.4 0.1 reshape.209
  20.5 0.6 reduce-window.6
  21.2 0.2 slice_reduce_fusion
  21.4 0.1 fusion.75
  21.5 0.2 select_reduce_fusion
  21.7 0.1 reduce_sum.67
  21.8 0.1 reshape.217
  22.0 0.2 fusion.32
  22.1 0.2 broadcast_in_dim.176
  22.3 0.0 copy-start.5
  22.3 23.3 %all-to-all-done = bf16[4,128,2048]{2,1,0:T(8,128)(2,1)S(1)} async-done(((bf16[4,128,2048]{2,1,0:T(8,128)(2,1)}), bf16[4,128,2048]{2,1,0:T(8,128)(2,1)S(1)}, u32[]{:S(2)}, u32[]{:S(2)}) %all-to-all-start) | async-done | bytes 2097184 | tf_op jit(solution)/shard_map/all_to_all | solution.py:23
  45.6 0.4 convert_reduce_fusion
  46.0 0.3 fusion.1
  46.2 0.2 fusion.3
  46.4 2.5 gather_fusion
  48.9 1.6 reshape.216
  50.5 1.8 select_bitcast_fusion
  52.4 62.8 %all_to_all.20 = bf16[64,1,6,2048]{3,2,1,0:T(8,128)(2,1)S(1)} all-to-all(bf16[64,1,6,2048]{3,2,1,0:T(8,128)(2,1)S(1)} %select_bitcast_fusion), channel_id=1, replica_groups=mesh['sp'=64,'tp'=4] {'sp'}, dimensions={0} | all-to-all | bytes 3145728 | tf_op jit(solution)/shard_map/all_to_all | solution.py:102
  115.1 2.0 copy.45
  117.2 0.6 collective-permute-start.2
  117.8 2.7 collective-permute-start.3
  120.4 32.9 %collective-permute-done.2 = bf16[64,1,6,2048]{3,0,2,1:T(8,128)(2,1)} collective-permute-done((bf16[64,1,6,2048]{3,0,2,1:T(8,128)(2,1)}, bf16[64,1,6,2048]{3,0,2,1:T(8,128)(2,1)}, u32[]{:S(2)}, u32[]{:S(2)}) %collective-permute-start.2) | collective-permute-done | bytes 1572896 | tf_op jit(solution)/shard_map/ppermute | solution.py:111
  153.3 0.0 collective-permute-start.4
  153.3 4.3 %broadcast_in_dim.175 = bf16[64,4,6,2048]{3,2,1,0:T(8,128)(2,1)} broadcast(bf16[]{:T(256)} %constant.139.clone.1), dimensions={} | broadcast | bytes 6291458 | tf_op jit(solution)/shard_map/broadcast_in_dim | solution.py:106
  157.6 1.5 constant_dynamic-update-slice_fusion
  159.2 3.6 copy_dynamic-update-slice_fusion.2
  162.7 3.6 copy_dynamic-update-slice_fusion.1
  166.3 22.3 %collective-permute-done.4 = bf16[64,1,6,2048]{3,0,2,1:T(8,128)(2,1)} collective-permute-done((bf16[64,1,6,2048]{3,0,2,1:T(8,128)(2,1)}, bf16[64,1,6,2048]{3,0,2,1:T(8,128)(2,1)}, u32[]{:S(2)}, u32[]{:S(2)}) %collective-permute-start.4) | collective-permute-done | bytes 1572896 | tf_op jit(solution)/shard_map/ppermute | solution.py:111
  188.6 3.6 copy_dynamic-update-slice_fusion
  192.3 11.1 %reshape.211 = bf16[1536,2048]{1,0:T(8,128)(2,1)} reshape(bf16[64,4,6,2048]{3,2,1,0:T(8,128)(2,1)} %copy_dynamic-update-slice_fusion) | data formatting | bytes 12582912 | tf_op jit(solution)/shard_map/reshape | solution.py:119
  203.4 4.8 %fusion.10 = f32[1536,256]{1,0:T(8,128)S(1)} fusion(bf16[1536,2048]{1,0:T(8,128)(2,1)} %reshape.211, bf16[1,2048,256]{2,1,0:T(8,128)(2,1)S(1)} %copy-done.7), kind=kOutput, calls=%fused_computation.24 | convolution fusion | flops 1610612736 | bytes 8912896 | tf_op jit(solution)/shard_map/dot_general | solution.py:120
  208.2 0.0 copy-done.8
  208.3 2.1 multiply_convert_fusion
  210.3 0.0 copy-start.3
  210.4 0.3 dot_general.21
  210.6 0.9 copy-done.3
  211.6 2.0 convert_bitcast_fusion
  213.6 71.0 %all_to_all.21 = bf16[4,64,1,6,2048]{4,1,3,2,0:T(8,128)(2,1)S(1)} all-to-all(bf16[4,64,1,6,2048]{4,1,3,2,0:T(8,128)(2,1)S(1)} %convert_bitcast_fusion), channel_id=1, replica_groups=mesh['sp'=64,'tp'=4] {'tp'}, dimensions={0} | all-to-all | bytes 12582912 | tf_op jit(solution)/shard_map/all_to_all | solution.py:23
  284.6 1.2 bitcast_reduce_fusion
  285.8 2.2 copy.53
  288.0 12.3 %all-to-all-start.3 = ((bf16[64,1,6,2048]{3,2,1,0:T(8,128)(2,1)}), bf16[64,1,6,2048]{3,2,1,0:T(8,128)(2,1)}, u32[]{:S(2)}, u32[]{:S(2)}) async-start(bf16[64,1,6,2048]{3,2,1,0:T(8,128)(2,1)} %copy.53), calls=%async_computation.3 | async-start | bytes 4194304 | tf_op jit(solution)/shard_map/all_to_all | solution.py:127
  300.3 0.1 copy.54
  300.4 0.1 mul.92
  300.6 0.1 copy.40
  300.7 50.8 %all-to-all-done.3 = bf16[64,1,6,2048]{3,2,1,0:T(8,128)(2,1)} async-done(((bf16[64,1,6,2048]{3,2,1,0:T(8,128)(2,1)}), bf16[64,1,6,2048]{3,2,1,0:T(8,128)(2,1)}, u32[]{:S(2)}, u32[]{:S(2)}) %all-to-all-start.3) | async-done | bytes 1572896 | tf_op jit(solution)/shard_map/all_to_all | solution.py:127
  351.5 2.6 reshape.213
  354.1 2.3 gather_fusion.1
  356.4 3.5 reshape.214
  360.0 4.8 %multiply_reduce_fusion = f32[128,2048]{1,0:T(8,128)S(1)} fusion(f32[128,2,2048]{2,1,0:T(2,128)} %reshape.214, f32[128,2]{1,0:T(8,128)S(1)} %copy.40), kind=kLoop, calls=%fused_computation.9 | loop fusion | flops 786432 | bytes 3146752 | tf_op jit(solution)/shard_map/reduce_sum | solution.py:130
  364.8 0.9 fusion.4
  (26 shorter events, 0.1 us)
Async XLA Ops:
  0.0 9.5 %copy-start = (bf16[512,2048]{1,0:T(8,128)(2,1)S(1)}, bf16[512,2048]{1,0:T(8,128)(2,1)}, u32[]{:S(2)}) copy-start(bf16[512,2048]{1,0:T(8,128)(2,1)} %param.17) | copy-start | bytes 6291460
  0.9 6.2 %collective-permute-start.1 = (bf16[15]{0:T(256)(128)(2,1)S(1)}, bf16[15]{0:T(256)(128)(2,1)S(1)}, u32[]{:S(2)}, u32[]{:S(2)}) collective-permute-start(bf16[15]{0:T(256)(128)(2,1)S(1)} %slice.108), channel_id=1, source_target_pairs={{0,4},{4,8},{8,12},{12,16},{16,20},{20,24},{24,28},{28,32},{32,36}... | collective-permute-start | bytes 98 | tf_op jit(solution)/shard_map/ppermute | solution.py:13
  3.6 5.0 %collective-permute-start = (bf16[15,256]{1,0:T(8,128)(2,1)S(1)}, bf16[15,256]{1,0:T(8,128)(2,1)S(1)}, u32[]{:S(2)}, u32[]{:S(2)}) collective-permute-start(bf16[15,256]{1,0:T(8,128)(2,1)S(1)} %slice.106), channel_id=1, source_target_pairs={{0,4},{4,8},{8,12},{12,16},{16,20},{20,24},{24,28},{28,32},{32,36}... | collective-permute-start | bytes 23048 | tf_op jit(solution)/shard_map/ppermute | solution.py:13
  14.9 30.6 %all-to-all-start = ((bf16[4,128,2048]{2,1,0:T(8,128)(2,1)}), bf16[4,128,2048]{2,1,0:T(8,128)(2,1)S(1)}, u32[]{:S(2)}, u32[]{:S(2)}) async-start(bf16[4,128,2048]{2,1,0:T(8,128)(2,1)} %bitcast.60), calls=%async_computation | async-start | bytes 4194304 | tf_op jit(solution)/shard_map/all_to_all | solution.py:23
  19.4 26.6 %copy-start.4 = (bf16[128,2048]{1,0:T(8,128)(2,1)S(1)}, bf16[128,2048]{1,0:T(8,128)(2,1)}, u32[]{:S(2)}) copy-start(bf16[128,2048]{1,0:T(8,128)(2,1)} %param.12) | copy-start | bytes 1572868
  22.3 23.9 %copy-start.5 = (f32[2048]{0:T(1024)S(1)}, f32[2048]{0:T(1024)}, u32[]{:S(2)}) copy-start(f32[2048]{0:T(1024)} %param.18) | copy-start | bytes 24580
  117.2 36.1 %collective-permute-start.2 = (bf16[64,1,6,2048]{3,0,2,1:T(8,128)(2,1)}, bf16[64,1,6,2048]{3,0,2,1:T(8,128)(2,1)}, u32[]{:S(2)}, u32[]{:S(2)}) collective-permute-start(bf16[64,1,6,2048]{3,0,2,1:T(8,128)(2,1)} %copy.45), channel_id=1, source_target_pairs={{0,1},{1,2},{2,3},{3,0},{4,5},{5,6},{6,7},{7,4},{8,9},{9,10},{10,1... | collective-permute-start | bytes 4718600 | tf_op jit(solution)/shard_map/ppermute | solution.py:111
  117.8 45.0 %collective-permute-start.3 = (bf16[64,1,6,2048]{3,0,2,1:T(8,128)(2,1)}, bf16[64,1,6,2048]{3,0,2,1:T(8,128)(2,1)}, u32[]{:S(2)}, u32[]{:S(2)}) collective-permute-start(bf16[64,1,6,2048]{3,0,2,1:T(8,128)(2,1)} %copy.45), channel_id=1, source_target_pairs={{0,3},{1,0},{2,1},{3,2},{4,7},{5,4},{6,5},{7,6},{8,11},{9,8},{10,9... | collective-permute-start | bytes 4718600 | tf_op jit(solution)/shard_map/ppermute | solution.py:114
  153.3 35.3 %collective-permute-start.4 = (bf16[64,1,6,2048]{3,0,2,1:T(8,128)(2,1)}, bf16[64,1,6,2048]{3,0,2,1:T(8,128)(2,1)}, u32[]{:S(2)}, u32[]{:S(2)}) collective-permute-start(bf16[64,1,6,2048]{3,0,2,1:T(8,128)(2,1)} %collective-permute-done.2), channel_id=1, source_target_pairs={{0,1},{1,2},{2,3},{3,0},{4,5},{5,6},{6,7},{7,4},{8,9},{9,10},{10,1... | collective-permute-start | bytes 4718600 | tf_op jit(solution)/shard_map/ppermute | solution.py:111
  192.3 11.1 %copy-start.7 = (bf16[1,2048,256]{2,1,0:T(8,128)(2,1)S(1)}, bf16[1,2048,256]{2,1,0:T(8,128)(2,1)}, u32[]{:S(2)}) copy-start(bf16[1,2048,256]{2,1,0:T(8,128)(2,1)} %param.21) | copy-start | bytes 3145732
  203.4 4.8 %copy-start.2 = (bf16[1536,2048]{1,0:T(8,128)(2,1)S(1)}, bf16[1536,2048]{1,0:T(8,128)(2,1)}, u32[]{:S(2)}) copy-start(bf16[1536,2048]{1,0:T(8,128)(2,1)} %reshape.211) | copy-start | bytes 18874372
  203.4 4.9 %copy-start.8 = (bf16[1,2048,256]{2,1,0:T(8,128)(2,1)S(1)}, bf16[1,2048,256]{2,1,0:T(8,128)(2,1)}, u32[]{:S(2)}) copy-start(bf16[1,2048,256]{2,1,0:T(8,128)(2,1)} %param.22) | copy-start | bytes 3145732
  210.3 1.2 copy-start.3
  288.0 12.6 %copy-start.6 = (f32[128,2]{0,1:T(2,128)S(1)}, f32[128,2]{0,1:T(2,128)}, u32[]{:S(2)}) copy-start(f32[128,2]{0,1:T(2,128)} %param.20) | copy-start | bytes 3076
  288.0 63.5 %all-to-all-start.3 = ((bf16[64,1,6,2048]{3,2,1,0:T(8,128)(2,1)}), bf16[64,1,6,2048]{3,2,1,0:T(8,128)(2,1)}, u32[]{:S(2)}, u32[]{:S(2)}) async-start(bf16[64,1,6,2048]{3,2,1,0:T(8,128)(2,1)} %copy.53), calls=%async_computation.3 | async-start | bytes 4194304 | tf_op jit(solution)/shard_map/all_to_all | solution.py:127
  356.4 9.3 %copy-start.1 = (bf16[512,2048]{1,0:T(8,128)(2,1)S(1)}, bf16[512,2048]{1,0:T(8,128)(2,1)}, u32[]{:S(2)}) copy-start(bf16[512,2048]{1,0:T(8,128)(2,1)} %param.17) | copy-start | bytes 6291460
